TPU v7x, 32 devices: a whole 2x2x4 slice. The times are simulated.
32 devices in a mesh: fs: 16 (over z, y, x), tp: 2 (over core).
Axes of the slice: x: 2, y: 2, z: 4, core: 2. Of those that a mesh axis runs over, the one named last changes fastest.
Arguments:
- tokens: bfloat16 [12288, 2048], P('fs'), may hold values from -6 to 6
- norm_gain: float32 [2048], replicated, may hold values from 0.1 to 1.9
- gate_weight: bfloat16 [2048, 5120], P('fs', 'tp'), may hold values from -0.125 to 0.125
- up_weight: bfloat16 [2048, 5120], P('fs', 'tp'), may hold values from -0.125 to 0.125
- down_weight: bfloat16 [5120, 2048], P('tp', 'fs'), may hold values from -0.078125 to 0.078125
Outputs:
- mixed: bfloat16 [12288, 2048], P(('fs', 'tp'))
All inputs are finite; a program needn't handle non-finite values.
Results may differ from a plain program's by a relative error of at most 0.014.
Values may be sent and summed in bfloat16 or wider, within the bound.
A program may use at most 128 MiB of HBM per device.

v0:
```python
import jax
import jax.numpy as jnp
from jax import lax
from jax.sharding import PartitionSpec as P


def add_rows(normed, piece):
    return jnp.dot(normed, piece, preferred_element_type=jnp.float32)


def per_device(tokens, norm_gain, gate_weight, up_weight, down_weight):
    values = tokens.astype(jnp.float32)
    scale = lax.rsqrt(jnp.mean(values * values, axis=-1, keepdims=True) + 1e-06)
    normed = (values * scale * norm_gain).astype(jnp.bfloat16)

    def add_single(piece):
        return add_rows(normed, piece)

    gate_proj = add_single(lax.all_gather(gate_weight, "fs", axis=0, tiled=True))
    up_proj = add_single(lax.all_gather(up_weight, "fs", axis=0, tiled=True))
    hidden = (jax.nn.silu(gate_proj) * up_proj).astype(jnp.bfloat16)
    down_whole = lax.all_gather(down_weight, "fs", axis=1, tiled=True)
    return lax.psum_scatter(
        jnp.dot(hidden, down_whole, preferred_element_type=jnp.float32).astype(jnp.bfloat16),
        "tp",
        scatter_dimension=0,
        tiled=True,
    )


def solution(mesh):
    in_specs = (P("fs", None), P(), P("fs", "tp"), P("fs", "tp"), P("tp", "fs"))
    out_specs = P(("fs", "tp"), None)
    return jax.shard_map(
        per_device, mesh=mesh, in_specs=in_specs, out_specs=out_specs, check_vma=False
    )
```

profile of v0, /device:TPU:0, one launch (start us, length us, event | category | flops | bytes accessed | tf_op | source)
XLA Modules:
  0.0 489.8 jit_solution(3628427633222220995)
XLA Ops:
  6.5 0.0 all-gather.4.cloned.1.call-start
  6.5 0.7 all-gather.4.cloned.1.call-update
  7.3 0.0 all-gather.6.cloned.1.call-start
  7.3 0.7 all-gather.6.cloned.1.call-update
  8.0 0.0 all-gather.8.cloned.1.call-start
  8.1 0.7 all-gather.8.cloned.1.call-update
  8.7 0.0 reduce-scatter.2.cloned.1.call-start
  8.8 2.6 fusion
  11.4 0.0 copy-start
  11.4 0.0 copy-start.1
  11.4 132.8 %all-gather.4.cloned.1.call-done = bf16[2048,2560]{1,0:T(8,128)(2,1)} async-done(((bf16[128,2560]{1,0:T(8,128)(2,1)}), bf16[2048,2560]{1,0:T(8,128)(2,1)}) %all-gather.4.cloned.1.call-update) | async-done | bytes 10485776 | tf_op jit(solution)/shard_map/all_gather | solution.py:19
  144.2 13.9 %fusion.5 = f32[768,2560]{1,0:T(8,128)} fusion(bf16[2048,2560]{1,0:T(8,128)(2,1)} %all-gather.4.cloned.1.call-done, bf16[768,2048]{1,0:T(8,128)(2,1)} %param.5, f32[2048]{0:T(1024)} %param.6, f32[768]{0:T(1024)S(1)} %add_rsqrt_fusion), kind=kOutput, calls=%fused_computation.7 | convolution fusion | flops 8059355136 | bytes 21507072 | tf_op jit(solution)/shard_map/dot_general | solution.py:8
  158.2 118.4 %all-gather.6.cloned.1.call-done = bf16[2048,2560]{1,0:T(8,128)(2,1)} async-done(((bf16[128,2560]{1,0:T(8,128)(2,1)}), bf16[2048,2560]{1,0:T(8,128)(2,1)}) %all-gather.6.cloned.1.call-update) | async-done | bytes 10485776 | tf_op jit(solution)/shard_map/all_gather | solution.py:20
  276.6 169.6 %all-gather.8.cloned.1.call-done = bf16[2560,2048]{1,0:T(8,128)(2,1)} async-done(((bf16[2560,128]{1,0:T(8,128)(2,1)}), bf16[2560,2048]{1,0:T(8,128)(2,1)}) %all-gather.8.cloned.1.call-update) | async-done | bytes 10485776 | tf_op jit(solution)/shard_map/all_gather | solution.py:22
  446.2 0.0 copy-done
  446.2 0.0 copy-done.1
  446.2 27.6 %convolution_convert_fusion = bf16[768,2048]{1,0:T(8,128)(2,1)} fusion(bf16[2560,2048]{1,0:T(8,128)(2,1)} %all-gather.8.cloned.1.call-done, f32[768,2560]{1,0:T(8,128)} %fusion.5, bf16[2048,2560]{1,0:T(8,128)(2,1)} %all-gather.6.cloned.1.call-done, bf16[768,2048]{1,0:T(8,128)(2,1)S(1)} %copy-done, f32[2048]{0:T(1024)S(1)} %copy-done.1, ...), kind=kOutput, calls=%fused_computation.6 | convolution fusion | flops 16125788160 | bytes 35138560 | tf_op jit(solution)/shard_map/dot_general | solution.py:24
  473.8 0.0 reduce-scatter.2.cloned.1.call-update
  473.8 9.5 %reduce-scatter.2.cloned.1.call-done = bf16[384,2048]{1,0:T(8,128)(2,1)} async-done(((bf16[768,2048]{1,0:T(8,128)(2,1)}), bf16[384,2048]{1,0:T(8,128)(2,1)}) %reduce-scatter.2.cloned.1.call-update) | async-done | bytes 1572880 | tf_op jit(solution)/shard_map/reduce_scatter | solution.py:23
  (1 shorter events, 0.0 us)
Async XLA Ops:
  6.5 137.7 %all-gather.4.cloned.1.call-start = ((), (), s32[]{:S(2)}) async-start(), calls=%async_computation.1 | async-start | bytes 11141120 | tf_op jit(solution)/shard_map/all_gather | solution.py:19
  7.3 269.4 %all-gather.6.cloned.1.call-start = ((), (), s32[]{:S(2)}) async-start(), calls=%async_computation.2 | async-start | bytes 11141120 | tf_op jit(solution)/shard_map/all_gather | solution.py:20
  8.0 438.2 %all-gather.8.cloned.1.call-start = ((), (), s32[]{:S(2)}) async-start(), calls=%async_computation.3 | async-start | bytes 11141120 | tf_op jit(solution)/shard_map/all_gather | solution.py:22
  8.7 474.6 %reduce-scatter.2.cloned.1.call-start = ((), (), s32[]{:S(2)}) async-start(), calls=%async_computation.4 | async-start | bytes 4718592 | tf_op jit(solution)/shard_map/reduce_scatter | solution.py:23
  11.4 434.8 %copy-start = (bf16[768,2048]{1,0:T(8,128)(2,1)S(1)}, bf16[768,2048]{1,0:T(8,128)(2,1)}, u32[]{:S(2)}) copy-start(bf16[768,2048]{1,0:T(8,128)(2,1)} %param.5) | copy-start | bytes 9437188
  11.4 434.8 %copy-start.1 = (f32[2048]{0:T(1024)S(1)}, f32[2048]{0:T(1024)}, u32[]{:S(2)}) copy-start(f32[2048]{0:T(1024)} %param.6) | copy-start | bytes 24580
Sparse Core Ops, SparseCore 0:
  10.0 134.1 all-gather.3
  146.9 129.6 all-gather.5
  279.3 166.8 all-gather.7
  473.9 9.3 reduce-scatter.1
where the time goes:
time: 490 us
  waiting for transfers between devices  432 us (88%)
  matrix products  41.5 us (8%)
  between operations  13.1 us (3%)
    all_gather x1, waiting for transfers between devices, per_device(): down_whole = lax.all_gather(down_weight, 'fs', axis=1, tiled=True)  170 us
    all_gather x1, waiting for transfers between devices, per_device(): lax.all_gather(gate_weight, 'fs', axis=0, tiled=True)  133 us
    all_gather x1, waiting for transfers between devices, per_device(): up_proj = add_single(lax.all_gather(up_weight, 'fs', axis=0, tiled=True))  118 us
    dot_general x1, matrix products, per_device(): jnp.dot(hidden, down_whole, preferred_element_type=jnp.float32)  27.6 us
    dot_general x1, matrix products, add_rows(): return jnp.dot(normed, piece, preferred_element_type=jnp.float32)  13.9 us
  transfers between devices with their start and end apart: 4, of which 4 were waited for; matrix products, arithmetic and copies ran while one was open for 3% of the time, Pallas kernels for 0%

commit v1 on v0

--- a/solution.py
+++ b/solution.py
@@ -19,7 +19,7 @@
     gate_proj = add_single(lax.all_gather(gate_weight, "fs", axis=0, tiled=True))
     up_proj = add_single(lax.all_gather(up_weight, "fs", axis=0, tiled=True))
     hidden = (jax.nn.silu(gate_proj) * up_proj).astype(jnp.bfloat16)
-    down_whole = lax.all_gather(down_weight, "fs", axis=1, tiled=True)
+    down_whole = jnp.concatenate(lax.all_gather(down_weight, "fs"), axis=1)
     return lax.psum_scatter(
         jnp.dot(hidden, down_whole, preferred_element_type=jnp.float32).astype(jnp.bfloat16),
         "tp",

time: 490 us -> 451 us (0.920)
  waiting for transfers between devices: 432 us -> 382 us
  local copies, waits for them, and re-layouts: 0.01 us -> 14.2 us
    all_gather x1, waiting for transfers between devices: 170 us -> 133 us  [per_device(): down_whole = jnp.concatenate(lax.all_gather(down_weight, 'fs'), axis=1)]
    all_gather x1, waiting for transfers between devices: 133 us -> 118 us  [per_device(): lax.all_gather(gate_weight, 'fs', axis=0, tiled=True)]
    reshape x0 -> x1, local copies, waits for them, and re-layouts: none -> 14.2 us  [per_device(): down_whole = jnp.concatenate(lax.all_gather(down_weight, 'fs'), axis=1)]
  transfers between devices with their start and end apart: 4 -> 4, of which waited for: 4 -> 4; matrix products, arithmetic and copies ran while one was open for 3% -> 7% of each run, Pallas kernels for 0% -> 0%
where the time goes in v1:
time: 451 us
  waiting for transfers between devices  382 us (85%)
  matrix products  38.9 us (9%)
  local copies, waits for them, and re-layouts  14.2 us (3%)
  between operations  13.1 us (3%)
    all_gather x1, waiting for transfers between devices, per_device(): down_whole = jnp.concatenate(lax.all_gather(down_weight, 'fs'), axis=1)  133 us
    all_gather x1, waiting for transfers between devices, per_device(): up_proj = add_single(lax.all_gather(up_weight, 'fs', axis=0, tiled=True))  119 us
    all_gather x1, waiting for transfers between devices, per_device(): lax.all_gather(gate_weight, 'fs', axis=0, tiled=True)  118 us
    dot_general x1, matrix products, per_device(): jnp.dot(hidden, down_whole, preferred_element_type=jnp.float32)  25.9 us
    reshape x1, local copies, waits for them, and re-layouts, per_device(): down_whole = jnp.concatenate(lax.all_gather(down_weight, 'fs'), axis=1)  14.2 us
    dot_general x1, matrix products, add_rows(): return jnp.dot(normed, piece, preferred_element_type=jnp.float32)  13 us
    reduce_scatter x1, waiting for transfers between devices, per_device(): lax.psum_scatter(jnp.dot(hidden, down_whole, preferred_element_type=jnp.f...  9.51 us
  transfers between devices with their start and end apart: 4, of which 4 were waited for; matrix products, arithmetic and copies ran while one was open for 7% of the time, Pallas kernels for 0%

profile of v1, /device:TPU:0, one launch (start us, length us, event | category | flops | bytes accessed | tf_op | source)
XLA Modules:
  0.0 451.0 jit_solution(9232343906918827705)
XLA Ops:
  6.5 0.0 all-gather.9.cloned.1.call-start
  6.5 0.7 all-gather.9.cloned.1.call-update
  7.3 0.0 all-gather.5.cloned.1.call-start
  7.3 0.7 all-gather.5.cloned.1.call-update
  8.0 0.0 all-gather.7.cloned.1.call-start
  8.1 0.7 all-gather.7.cloned.1.call-update
  8.7 0.0 reduce-scatter.2.cloned.1.call-start
  8.8 2.6 fusion
  11.4 132.9 %all-gather.9.cloned.1.call-done = bf16[40960,128]{1,0:T(8,128)(2,1)} async-done(((bf16[2560,128]{1,0:T(8,128)(2,1)}), bf16[40960,128]{1,0:T(8,128)(2,1)}) %all-gather.9.cloned.1.call-update) | async-done | bytes 10485776 | tf_op jit(solution)/shard_map/all_gather | solution.py:22
  144.2 0.0 copy-start
  144.2 0.0 copy-start.1
  144.2 14.2 %copy.6 = bf16[2560,16,128]{0,2,1:T(8,128)(2,1)} copy(bf16[2560,16,128]{2,0,1:T(8,128)(2,1)} %bitcast.7) | data formatting | bytes 20971520 | tf_op jit(solution)/shard_map/reshape | solution.py:22
  158.4 118.2 %all-gather.5.cloned.1.call-done = bf16[2048,2560]{1,0:T(8,128)(2,1)} async-done(((bf16[128,2560]{1,0:T(8,128)(2,1)}), bf16[2048,2560]{1,0:T(8,128)(2,1)}) %all-gather.5.cloned.1.call-update) | async-done | bytes 10485776 | tf_op jit(solution)/shard_map/all_gather | solution.py:19
  276.6 0.0 copy-done
  276.6 0.0 copy-done.1
  276.6 13.0 %fusion.5 = f32[768,2560]{1,0:T(8,128)} fusion(bf16[2048,2560]{1,0:T(8,128)(2,1)} %all-gather.5.cloned.1.call-done, bf16[768,2048]{1,0:T(8,128)(2,1)S(1)} %copy-done, f32[2048]{0:T(1024)S(1)} %copy-done.1, f32[768]{0:T(1024)S(1)} %add_rsqrt_fusion), kind=kOutput, calls=%fused_computation.7 | convolution fusion | flops 8059355136 | bytes 21507072 | tf_op jit(solution)/shard_map/dot_general | solution.py:8
  289.6 119.4 %all-gather.7.cloned.1.call-done = bf16[2048,2560]{1,0:T(8,128)(2,1)} async-done(((bf16[128,2560]{1,0:T(8,128)(2,1)}), bf16[2048,2560]{1,0:T(8,128)(2,1)}) %all-gather.7.cloned.1.call-update) | async-done | bytes 10485776 | tf_op jit(solution)/shard_map/all_gather | solution.py:20
  409.0 25.9 %convolution_convert_fusion = bf16[768,2048]{1,0:T(8,128)(2,1)} fusion(bf16[2560,2048]{0,1:T(8,128)(2,1)} %bitcast.8, f32[768,2560]{1,0:T(8,128)} %fusion.5, bf16[2048,2560]{1,0:T(8,128)(2,1)} %all-gather.7.cloned.1.call-done, bf16[768,2048]{1,0:T(8,128)(2,1)S(1)} %copy-done, f32[2048]{0:T(1024)S(1)} %copy-done.1, f32[768]{0:T(1024)S(1)} %add_rsqrt_fusion), kind=kOutput, calls=%fused_computation.6 | convolution fusion | flops 16125788160 | bytes 35138560 | tf_op jit(solution)/shard_map/dot_general | solution.py:24
  434.9 0.0 reduce-scatter.2.cloned.1.call-update
  434.9 9.5 %reduce-scatter.2.cloned.1.call-done = bf16[384,2048]{1,0:T(8,128)(2,1)} async-done(((bf16[768,2048]{1,0:T(8,128)(2,1)}), bf16[384,2048]{1,0:T(8,128)(2,1)}) %reduce-scatter.2.cloned.1.call-update) | async-done | bytes 1572880 | tf_op jit(solution)/shard_map/reduce_scatter | solution.py:23
  (1 shorter events, 0.0 us)
Async XLA Ops:
  6.5 137.7 %all-gather.9.cloned.1.call-start = ((), (), s32[]{:S(2)}) async-start(), calls=%async_computation.4 | async-start | bytes 11141120 | tf_op jit(solution)/shard_map/all_gather | solution.py:22
  7.3 269.4 %all-gather.5.cloned.1.call-start = ((), (), s32[]{:S(2)}) async-start(), calls=%async_computation.1 | async-start | bytes 11141120 | tf_op jit(solution)/shard_map/all_gather | solution.py:19
  8.0 401.0 %all-gather.7.cloned.1.call-start = ((), (), s32[]{:S(2)}) async-start(), calls=%async_computation.2 | async-start | bytes 11141120 | tf_op jit(solution)/shard_map/all_gather | solution.py:20
  8.7 435.7 %reduce-scatter.2.cloned.1.call-start = ((), (), s32[]{:S(2)}) async-start(), calls=%async_computation.3 | async-start | bytes 4718592 | tf_op jit(solution)/shard_map/reduce_scatter | solution.py:23
  144.2 132.4 %copy-start = (bf16[768,2048]{1,0:T(8,128)(2,1)S(1)}, bf16[768,2048]{1,0:T(8,128)(2,1)}, u32[]{:S(2)}) copy-start(bf16[768,2048]{1,0:T(8,128)(2,1)} %param.5) | copy-start | bytes 9437188
  144.2 132.4 %copy-start.1 = (f32[2048]{0:T(1024)S(1)}, f32[2048]{0:T(1024)}, u32[]{:S(2)}) copy-start(f32[2048]{0:T(1024)} %param.6) | copy-start | bytes 24580
Sparse Core Ops, SparseCore 0:
  10.0 134.1 all-gather.8
  146.9 129.6 all-gather.4
  279.3 129.6 all-gather.6
  435.0 9.3 reduce-scatter.1
